TPU v7x, 32 devices: a whole 2x2x4 slice. The times are simulated.
32 devices in a mesh: sp: 4 (over z), tp: 2 (over y), dp: 4 (over x, core).
Axes of the slice: x: 2, y: 2, z: 4, core: 2. Of those that a mesh axis runs over, the one named last changes fastest.
Arguments:
- latent: bfloat16 [2048, 2048], P(('dp', 'sp', 'tp')), parts along dimension 0, may hold values from -6 to 6
- cond: bfloat16 [8192], P('dp'), parts along dimension 0, may hold values from -6 to 6
- context: bfloat16 [2048, 2048], P(('dp', 'sp')), parts along dimension 0, may hold values from -6 to 6
- context_cond: bfloat16 [2048], replicated, may hold values from -6 to 6
- modulation: bfloat16 [2048, 6144], P(('sp', 'tp')), may hold values from -0.125 to 0.125
- norm_gain: bfloat16 [2048], replicated, may hold values from 0.099609375 to 1.8984375
- w_x: bfloat16 [2048, 1024], P(None, 'tp'), may hold values from -0.125 to 0.125
- w_gate: bfloat16 [2048, 1024], P(None, 'tp'), may hold values from -0.125 to 0.125
- w_b: bfloat16 [2048, 256], P(None, 'tp'), may hold values from -0.125 to 0.125
- w_c: bfloat16 [2048, 256], P(None, 'tp'), may hold values from -0.125 to 0.125
- w_dt: bfloat16 [2, 2048, 16], P(None, None, 'tp'), may hold values from -0.125 to 0.125
- conv_x: bfloat16 [4, 1024], P(None, 'tp'), may hold values from -3 to 3
- conv_b: bfloat16 [4, 256], P(None, 'tp'), may hold values from -3 to 3
- conv_c: bfloat16 [4, 256], P(None, 'tp'), may hold values from -3 to 3
- decay_rate: float32 [2, 16], P(None, 'tp'), may hold values from 0 to 0.04
- decay_extra: float32 [2048, 16], P(('dp', 'sp'), 'tp'), parts along dimension 0, may hold values from -2 to 0
- out_gain: bfloat16 [1024], P('tp'), may hold values from 0.099609375 to 1.8984375
- w_out: bfloat16 [1024, 2048], replicated, may hold values from -0.1875 to 0.1875
Outputs:
- mixed: bfloat16 [2048, 2048], P(('dp', 'sp', 'tp')), parts along dimension 0
There are 4 independent parts, one for each index of `dp`. A program takes and returns all parts, laid end to end along the dimension named above; an argument that names none is the same for every part. Nothing has to cross between parts.
All inputs are finite; a program needn't handle non-finite values.
Results may differ from a plain program's by a relative error of at most 0.007.
Values may be sent and summed in bfloat16 or wider, within the bound.
A program may use at most 64 MiB of HBM per device.

v0:
```python
import jax
import jax.numpy as jnp
from jax import lax
from jax.sharding import PartitionSpec as P

HEAD_DIM = 64
STATE = 64
BLOCK = 128


ROW_EPS = 1e-06
GROUP_EPS = 1e-05
HIGHEST = lax.Precision.HIGHEST


def prefix(x, axis, join, neutral, backward):
    count = lax.axis_size(axis)
    place = lax.axis_index(axis)
    ahead = count - 1 - place if backward else place
    gathered = jax.tree.map(
        lambda a, kind: lax.all_gather(a.astype(kind), axis),
        x,
        jax.tree.map(lambda a: jnp.bfloat16 if a.dtype == jnp.float32 else a.dtype, x),
    )
    state = jax.tree.map(lambda a, e: jnp.zeros_like(a) + jnp.asarray(e, a.dtype), x, neutral)

    def one(hop, state):
        source = count - 1 - hop if backward else hop
        return join(
            state,
            jax.tree.map(
                lambda a, own: lax.dynamic_index_in_dim(a, source, 0, False).astype(own.dtype),
                gathered,
                x,
            ),
        )

    return lax.fori_loop(0, ahead, one, state)


def with_halo(block, sides, width):
    for axis, dim in sides:
        count = lax.axis_size(axis)
        forward = [(i, i + 1) for i in range(count - 1)]
        backward = [(target, source) for source, target in forward]
        low = lax.ppermute(
            lax.slice_in_dim(block, block.shape[dim] - width, None, axis=dim), axis, forward
        )
        high = lax.ppermute(lax.slice_in_dim(block, 0, width, axis=dim), axis, backward)
        block = jnp.concatenate([low, block, high], axis=dim)
    return block


def modulated_norm(row_block, norm_gain, shift_row, scale_row):
    values = row_block.astype(jnp.float32)
    normed = values * lax.rsqrt(jnp.mean(values * values, axis=-1, keepdims=True) + ROW_EPS)
    return (normed * norm_gain.astype(jnp.float32) * (1.0 + scale_row) + shift_row).astype(
        jnp.bfloat16
    )


def project_many(row_block, weights):
    return jnp.concatenate(
        [
            jnp.dot(row_block, weight, preferred_element_type=jnp.float32).astype(jnp.bfloat16)
            for weight in weights
        ],
        axis=1,
    )


def conv_padded(padded, conv_taps, length):
    values = padded.astype(jnp.float32)
    summed = jnp.zeros((length, values.shape[1]), jnp.float32)
    for offset in range(conv_taps.shape[0]):
        summed = summed + conv_taps[offset].astype(jnp.float32) * values[offset : offset + length]
    return jax.nn.silu(summed).astype(jnp.bfloat16)


def context_states(ctx_xs, ctx_bmat, ctx_dt, decay_rate):
    length = ctx_xs.shape[0]
    groups = ctx_bmat.shape[1] // STATE
    heads_here = ctx_dt.shape[2]
    repeat = heads_here // groups
    values = ctx_xs.astype(jnp.float32).reshape(length, groups, repeat, HEAD_DIM)
    keys_b = ctx_bmat.astype(jnp.float32).reshape(length, groups, STATE)
    log_decay = -decay_rate[:, None, :] * ctx_dt
    running = jnp.cumsum(log_decay, axis=1)
    forward_weight = (jnp.exp(running[0, -1:] - running[0]) * ctx_dt[0]).reshape(
        length, groups, repeat
    )
    backward_weight = (jnp.exp(running[1] - log_decay[1]) * ctx_dt[1]).reshape(
        length, groups, repeat
    )
    forward_state = jnp.einsum(
        "lgn,lgr,lgrp->grpn", keys_b, forward_weight, values, precision=HIGHEST
    )
    backward_state = jnp.einsum(
        "lgn,lgr,lgrp->grpn", keys_b, backward_weight, values, precision=HIGHEST
    )
    return (forward_state, backward_state)


def block_pass(inputs, step_sizes, log_decay, bmat, cmat, start_state):
    length = inputs.shape[0]
    groups, repeat = (start_state.shape[0], start_state.shape[1])
    block_count = length // BLOCK
    values = inputs.reshape(block_count, BLOCK, groups, repeat, HEAD_DIM)
    steps_blk = step_sizes.reshape(block_count, BLOCK, groups, repeat)
    decays = log_decay.reshape(block_count, BLOCK, groups, repeat)
    keys_b = bmat.reshape(block_count, BLOCK, groups, STATE)
    reads_c = cmat.reshape(block_count, BLOCK, groups, STATE)
    lower_mask = (jnp.arange(BLOCK)[:, None] >= jnp.arange(BLOCK)[None, :])[:, :, None, None]

    def advance(carried, block_data):
        value_blk, step_blk, decay_blk, key_blk, read_blk = block_data
        running = jnp.cumsum(decay_blk, axis=0)
        log_gaps = running[:, None] - running[None, :]
        mixing = jnp.where(lower_mask, jnp.exp(jnp.where(lower_mask, log_gaps, 0.0)), 0.0)
        affinity = jnp.einsum("ign,jgn->ijg", read_blk, key_blk, preferred_element_type=jnp.float32)
        weights = (affinity[..., None] * mixing * step_blk[None]).astype(jnp.bfloat16)
        output = jnp.einsum(
            "ijgr,jgrp->igrp", weights, value_blk, preferred_element_type=jnp.float32
        )
        output = output + jnp.einsum(
            "ign,grpn,igr->igrp",
            read_blk.astype(jnp.float32),
            carried,
            jnp.exp(running),
            precision=HIGHEST,
        )
        to_end = jnp.exp(running[-1:] - running) * step_blk
        state_in = (key_blk.astype(jnp.float32)[:, :, None, :] * to_end[..., None]).astype(
            jnp.bfloat16
        )
        carried = jnp.exp(running[-1])[..., None, None] * carried + jnp.einsum(
            "jgrn,jgrp->grpn", state_in, value_blk, preferred_element_type=jnp.float32
        )
        return (carried, output)

    final_state, outputs = lax.scan(
        advance, start_state, (values, steps_blk, decays, keys_b, reads_c)
    )
    return (outputs.reshape(length, groups, repeat, HEAD_DIM), final_state)


def state_chain(summary, backward):

    def combine(earlier, later_part):
        return (
            earlier[0] + later_part[0],
            jnp.exp(later_part[0])[..., None, None] * earlier[1] + later_part[1],
        )

    identity_pair = (jnp.zeros_like(summary[0]), jnp.zeros_like(summary[1]))
    return prefix(summary, "sp", combine, identity_pair, backward)


def directed_pass(inputs, step_sizes, log_decay, bmat, cmat, outer_start, zeros_state, backward):
    local_out, final_state = block_pass(inputs, step_sizes, log_decay, bmat, cmat, zeros_state)
    length = inputs.shape[0]
    groups, repeat = (zeros_state.shape[0], zeros_state.shape[1])
    running = jnp.cumsum(log_decay, axis=0).reshape(length, groups, repeat)
    before = state_chain((running[-1], final_state), backward)
    entry_state = jnp.exp(before[0])[..., None, None] * outer_start + before[1]
    read_rows = cmat.astype(jnp.float32).reshape(length, groups, STATE)
    return local_out + jnp.einsum(
        "tgn,grpn,tgr->tgrp", read_rows, entry_state, jnp.exp(running), precision=HIGHEST
    )


def group_norm(combined, out_gain):
    length, groups, repeat, _ = combined.shape
    mean_square = jnp.mean(combined * combined, axis=(2, 3), keepdims=True)
    scaled = (
        combined
        * lax.rsqrt(mean_square + GROUP_EPS)
        * out_gain.astype(jnp.float32).reshape(groups, repeat, HEAD_DIM)
    )
    return scaled.reshape(length, groups * repeat * HEAD_DIM).astype(jnp.bfloat16)


def local(
    latent,
    cond,
    context,
    context_cond,
    modulation,
    norm_gain,
    w_x,
    w_gate,
    w_b,
    w_c,
    w_dt,
    conv_x,
    conv_b,
    conv_c,
    decay_rate,
    decay_extra,
    out_gain,
    w_out,
):
    model_width = latent.shape[1]
    mod_share = modulation.shape[0]
    cond_rows = jax.nn.silu(jnp.stack([cond, context_cond]).astype(jnp.float32)).astype(
        jnp.bfloat16
    )
    own_cols = lax.dynamic_slice_in_dim(
        cond_rows, lax.axis_index(("sp", "tp")) * mod_share, mod_share, 1
    )
    mod_rows = lax.psum(
        jnp.dot(own_cols, modulation, preferred_element_type=jnp.float32), ("sp", "tp")
    )
    shift_rows = mod_rows[:, :model_width]
    scale_rows = mod_rows[:, model_width : 2 * model_width]
    gate_row = mod_rows[0, 2 * model_width :]
    head_cols = w_x.shape[1]
    state_cols = w_b.shape[1]
    heads_here = w_dt.shape[2]
    groups_here = state_cols // STATE
    repeat = heads_here // groups_here
    hidden = modulated_norm(latent, norm_gain, shift_rows[0], scale_rows[0])
    latent_mats = (w_x, w_b, w_c, w_gate, w_dt[0], w_dt[1])
    projected = project_many(lax.all_gather(hidden, "tp", axis=0, tiled=True), latent_mats)
    token_count = projected.shape[0]
    conv_cols = head_cols + 2 * state_cols
    extended = with_halo(projected[:, :conv_cols], (("sp", 0),), 2)
    conv_taps = jnp.concatenate([conv_x, conv_b, conv_c], axis=1)
    convolved = conv_padded(extended, conv_taps, token_count)
    latent_xs = convolved[:, :head_cols]
    latent_b = convolved[:, head_cols : head_cols + state_cols]
    latent_c = convolved[:, head_cols + state_cols :]
    gate_in = projected[:, conv_cols : conv_cols + head_cols]
    dt_start = conv_cols + head_cols
    latent_dt = jnp.stack(
        [
            jax.nn.softplus(projected[:, dt_start : dt_start + heads_here].astype(jnp.float32)),
            jax.nn.softplus(projected[:, dt_start + heads_here :].astype(jnp.float32)),
        ]
    )
    context_mats = (w_x, w_b, w_dt[0], w_dt[1])
    own_context = project_many(
        modulated_norm(context, norm_gain, shift_rows[1], scale_rows[1]), context_mats
    )
    context_cols = lax.all_gather(own_context, "sp", axis=0, tiled=True)
    ctx_span = head_cols + state_cols
    ctx_padded = jnp.pad(context_cols[:, :ctx_span], ((2, 1), (0, 0)))
    ctx_conv = conv_padded(
        ctx_padded, jnp.concatenate([conv_x, conv_b], axis=1), context_cols.shape[0]
    )
    ctx_dt = jnp.stack(
        [
            jax.nn.softplus(context_cols[:, ctx_span : ctx_span + heads_here].astype(jnp.float32)),
            jax.nn.softplus(context_cols[:, ctx_span + heads_here :].astype(jnp.float32)),
        ]
    )
    forward_start, backward_start = context_states(
        ctx_conv[:, :head_cols], ctx_conv[:, head_cols:], ctx_dt, decay_rate
    )
    log_decay = -decay_rate[:, None, :] * latent_dt + decay_extra[None]
    zeros_state = jnp.zeros((groups_here, repeat, HEAD_DIM, STATE), jnp.float32)
    y_forward = directed_pass(
        latent_xs, latent_dt[0], log_decay[0], latent_b, latent_c, forward_start, zeros_state, False
    )
    y_backward = directed_pass(
        latent_xs[::-1],
        latent_dt[1][::-1],
        log_decay[1][::-1],
        latent_b[::-1],
        latent_c[::-1],
        backward_start,
        zeros_state,
        True,
    )
    gate_act = jax.nn.silu(gate_in.astype(jnp.float32)).reshape(
        token_count, groups_here, repeat, HEAD_DIM
    )
    combined = (y_forward + y_backward[::-1]) * gate_act
    normed = group_norm(combined, out_gain)
    tp_count = lax.axis_size("tp")
    stacked = normed.reshape(tp_count, token_count // tp_count, normed.shape[1])
    branch = jnp.dot(
        lax.all_to_all(stacked, "tp", split_axis=0, concat_axis=2, tiled=True)[0],
        w_out,
        preferred_element_type=jnp.float32,
    )[None]
    return (latent.astype(jnp.float32) + gate_row * branch[0]).astype(jnp.bfloat16)


def solution(mesh):
    in_specs = (
        P(("dp", "sp", "tp"), None),
        P("dp"),
        P(("dp", "sp"), None),
        P(),
        P(("sp", "tp"), None),
        P(),
        P(None, "tp"),
        P(None, "tp"),
        P(None, "tp"),
        P(None, "tp"),
        P(None, None, "tp"),
        P(None, "tp"),
        P(None, "tp"),
        P(None, "tp"),
        P(None, "tp"),
        P(("dp", "sp"), "tp"),
        P("tp"),
        P(),
    )
    out_specs = P(("dp", "sp", "tp"), None)
    return jax.shard_map(local, mesh=mesh, in_specs=in_specs, out_specs=out_specs, check_vma=False)
```

profile of v0, /device:TPU:0, one launch (start us, length us, event | category | flops | bytes accessed | tf_op | source)
XLA Modules:
  0.0 247.8 jit_solution(15845269503590403432)
XLA Ops:
  2.4 39.4 %psum.7 = f32[2,6144]{1,0:T(2,128)S(1)} all-reduce(f32[2,6144]{1,0:T(2,128)S(1)} %fusion.93), channel_id=1, replica_groups=mesh['sp'=4,'tp'=2,'dp'=4] {'sp','tp'}, use_global_device_ids=true, to_apply=%region_0.1 | all-reduce | flops 12288 | bytes 98304 | tf_op jit(solution)/shard_map/psum | solution.py:211
  42.9 7.2 %all_gather.26 = bf16[128,2048]{1,0:T(8,128)(2,1)S(1)} all-gather(bf16[64,2048]{1,0:T(8,128)(2,1)S(1)} %fusion.31), channel_id=1, replica_groups=mesh['sp'=4,'tp'=2,'dp'=4] {'tp'}, dimensions={0}, use_global_device_ids=true | all-gather | bytes 786432 | tf_op jit(solution)/shard_map/all_gather | solution.py:224
  50.0 2.3 convolution_convert_fusion.2
  53.6 1.9 collective-permute-start
  60.7 2.9 %convolution_convert_fusion.1 = bf16[128,512]{0,1:T(8,128)(2,1)S(1)} fusion(bf16[2048,512]{1,0:T(8,128)(2,1)} %param.28, bf16[128,2048]{1,0:T(8,128)(2,1)} %param.24, f32[2048]{0:T(1024)} %bitcast.249, f32[2048]{0:T(1024)} %bitcast.253, f32[2048]{0:T(1024)S(1)} %convert_element_type.221, f32[128]{0:T(128)S(1)} %add_rsqrt_fusion.1), kind=kOutput, calls=%fused_computation.49 | convolution fusion | flops 270073856 | bytes 2777600 | tf_op jit(solution)/shard_map/dot_general | solution.py:65
  65.2 14.5 %all_gather.30 = bf16[512,656]{0,1:T(8,128)(2,1)S(1)} all-gather(bf16[128,656]{0,1:T(8,128)(2,1)S(1)} %pad_maximum_fusion), channel_id=1, replica_groups=mesh['sp'=4,'tp'=2,'dp'=4] {'sp'}, dimensions={0}, use_global_device_ids=true | all-gather | bytes 839680 | tf_op jit(solution)/shard_map/all_gather | solution.py:245
  93.7 5.0 %reduce-window.6 = f32[2,8,4,128]{3,1,2,0:T(8,128)} reduce-window(f32[2,8,4,128]{3,1,2,0:T(8,128)} %fusion.148, f32[]{:T(128)} %constant.128.clone.1), window={size=1x1x1x128 pad=0_0x0_0x0_0x127_0}, to_apply=%region_7.8 | reduce-window | flops 1040384 | bytes 65540 | tf_op jit(solution)/shard_map/reduce-window
  103.1 2.7 %pad_convert_fusion = f32[515,640]{0,1:T(8,128)} fusion(bf16[512,640]{0,1:T(8,128)(2,1)} %slice.222), kind=kLoop, calls=%fused_computation.67 | loop fusion | flops 329600 | bytes 1973760 | tf_op jit(solution)/shard_map/convert_element_type | solution.py:73
  110.2 3.1 %divide_multiply_fusion = f32[128,512]{1,0:T(8,128)} fusion(bf16[128,2048]{1,0:T(8,128)(2,1)} %copy-done.2, bf16[2048,512]{1,0:T(8,128)(2,1)} %param.29), kind=kOutput, calls=%fused_computation.89 | convolution fusion | flops 268828672 | bytes 2883584 | tf_op jit(solution)/shard_map/dot_general | solution.py:65
  116.3 2.4 multiply_convert_fusion
  118.7 10.4 %all_gather.27 = bf16[4,2,4]{2,1,0:T(2,128)(2,1)} all-gather(bf16[1,2,4]{2,1,0:T(2,128)(2,1)S(1)} %copy-done.55), channel_id=1, replica_groups=mesh['sp'=4,'tp'=2,'dp'=4] {'sp'}, dimensions={0}, use_global_device_ids=true | all-gather | bytes 80 | tf_op jit(solution)/shard_map/all_gather | solution.py:21
  129.1 8.0 %all_gather.31 = bf16[4,2,4]{2,1,0:T(2,128)(2,1)} all-gather(bf16[1,2,4]{2,1,0:T(2,128)(2,1)S(1)} %copy-done.56), channel_id=1, replica_groups=mesh['sp'=4,'tp'=2,'dp'=4] {'sp'}, dimensions={0}, use_global_device_ids=true | all-gather | bytes 80 | tf_op jit(solution)/shard_map/all_gather | solution.py:21
  137.1 1.9 slice.230
  156.2 1.8 copy.190
  164.3 16.6 %all-gather = bf16[8,4,64,64]{3,2,1,0:T(8,128)(2,1)} all-gather(bf16[2,4,64,64]{3,2,1,0:T(8,128)(2,1)S(1)} %fusion.17), channel_id=2, replica_groups=mesh['sp'=4,'tp'=2,'dp'=4] {'sp'}, dimensions={0}, use_global_device_ids=true | all-gather | bytes 327680 | tf_op jit(solution)/shard_map/all_gather | solution.py:21
  182.7 1.6 copy.178
  187.7 19.2 %all-gather.1 = bf16[8,4,64,64]{3,2,1,0:T(8,128)(2,1)} all-gather(bf16[2,4,64,64]{3,2,1,0:T(8,128)(2,1)S(1)} %fusion.18), channel_id=3, replica_groups=mesh['sp'=4,'tp'=2,'dp'=4] {'sp'}, dimensions={0}, use_global_device_ids=true | all-gather | bytes 327680 | tf_op jit(solution)/shard_map/all_gather | solution.py:21
  207.5 7.0 %while.7 = (s32[]{:T(128)}, f32[2,4]{1,0:T(2,128)}, f32[2,4,64,64]{3,2,1,0:T(8,128)S(1)}, s32[]{:T(128)}, bf16[4,2,4]{2,1,0:T(2,128)(2,1)}, /*index=5*/bf16[4,2,...) while((s32[]{:T(128)}, f32[2,4]{1,0:T(2,128)}, f32[2,4,64,64]{3,2,1,0:T(8,128)S(1)}, ...), condition=%wide.region_12.13_spmd, body=%wide.region_11.12_spmd.sunk | while | flops 98326 | bytes 327979 | solution.py:38
  221.6 1.7 fusion.15
  225.5 1.8 rev.23
  229.0 1.7 copy.168
  231.7 1.7 fusion.16
  237.0 6.8 %all_to_all.15 = bf16[2,64,512]{2,1,0:T(8,128)(2,1)S(1)} all-to-all(bf16[2,64,512]{2,1,0:T(8,128)(2,1)S(1)} %copy.199), channel_id=1, replica_groups=mesh['sp'=4,'tp'=2,'dp'=4] {'tp'}, dimensions={0} | all-to-all | bytes 262144 | tf_op jit(solution)/shard_map/all_to_all | solution.py:283
  244.1 3.8 %fusion.1 = bf16[64,2048]{1,0:T(8,128)(2,1)} fusion(bf16[64,1024]{1,0:T(8,128)(2,1)S(1)} %bitcast.213, bf16[1024,2048]{1,0:T(8,128)(2,1)} %param.39, bf16[64,2048]{1,0:T(8,128)(2,1)S(1)} %copy-done.7, f32[2048]{0:T(1024)S(1)} %bitcast.239), kind=kOutput, calls=%fused_computation.10 | convolution fusion | flops 268959744 | bytes 4857856 | tf_op jit(solution)/shard_map/dot_general | solution.py:282
  (238 shorter events, 88.6 us)
Async XLA Ops:
  1.9 40.6 %copy-start.48 = (bf16[2048]{0:T(1024)(128)(2,1)S(1)}, bf16[2048]{0:T(1024)(128)(2,1)}, u32[]{:S(2)}) copy-start(bf16[2048]{0:T(1024)(128)(2,1)} %param.27) | copy-start | bytes 12292
  1.9 40.6 %copy-start.6 = (bf16[64,2048]{1,0:T(8,128)(2,1)S(1)}, bf16[64,2048]{1,0:T(8,128)(2,1)}, u32[]{:S(2)}) copy-start(bf16[64,2048]{1,0:T(8,128)(2,1)} %param.22) | copy-start | bytes 786436
  42.8 9.4 %copy-start.11 = (bf16[2048,128]{1,0:T(8,128)(2,1)S(1)}, bf16[2048,128]{1,0:T(8,128)(2,1)}, u32[]{:S(2)}) copy-start(bf16[2048,128]{1,0:T(8,128)(2,1)} %param.31) | copy-start | bytes 1572868
  50.0 7.0 %copy-start.2 = (bf16[128,2048]{1,0:T(8,128)(2,1)}, bf16[128,2048]{1,0:T(8,128)(2,1)S(1)}, u32[]{:S(2)}) copy-start(bf16[128,2048]{1,0:T(8,128)(2,1)S(1)} %all_gather.26) | copy-start | bytes 1572868
  53.6 105.8 %collective-permute-start = (bf16[2,768]{1,0:T(2,128)(2,1)}, bf16[2,768]{1,0:T(2,128)(2,1)}, u32[]{:S(2)}, u32[]{:S(2)}) collective-permute-start(bf16[2,768]{1,0:T(2,128)(2,1)} %get-tuple-element.220), channel_id=1, source_target_pairs={{0,8},{8,16},{16,24},{1,9},{9,17},{17,25},{2,10},{10,18},{18,26},{... | collective-permute-start | bytes 9224 | tf_op jit(solution)/shard_map/ppermute | solution.py:46
  55.4 103.9 %collective-permute-start.1 = (bf16[2,768]{1,0:T(2,128)(2,1)}, bf16[2,768]{1,0:T(2,128)(2,1)}, u32[]{:S(2)}, u32[]{:S(2)}) collective-permute-start(bf16[2,768]{1,0:T(2,128)(2,1)} %get-tuple-element.221), channel_id=1, source_target_pairs={{8,0},{16,8},{24,16},{9,1},{17,9},{25,17},{10,2},{18,10},{26,18},{... | collective-permute-start | bytes 9224 | tf_op jit(solution)/shard_map/ppermute | solution.py:49
  57.0 29.6 %copy-start.25 = (f32[128,8]{0,1:T(8,128)}, f32[128,8]{0,1:T(8,128)S(1)}, u32[]{:S(2)}) copy-start(f32[128,8]{0,1:T(8,128)S(1)} %compare_select_fusion.3) | copy-start | bytes 12292
  64.8 14.9 %copy-start.37 = (f32[2,8]{1,0:T(2,128)S(1)}, f32[2,8]{1,0:T(2,128)}, u32[]{:S(2)}) copy-start(f32[2,8]{1,0:T(2,128)} %copy-done.36) | copy-start | bytes 196
  65.2 17.6 %copy-start.41 = (f32[128,8]{0,1:T(8,128)S(1)}, f32[128,8]{0,1:T(8,128)}, u32[]{:S(2)}) copy-start(f32[128,8]{0,1:T(8,128)} %get-tuple-element.233) | copy-start | bytes 12292
  65.2 24.9 %copy-start.38 = (f32[128,8]{0,1:T(8,128)S(1)}, f32[128,8]{0,1:T(8,128)}, u32[]{:S(2)}) copy-start(f32[128,8]{0,1:T(8,128)} %get-tuple-element.232) | copy-start | bytes 12292
  110.2 6.1 %copy-start.1 = (f32[515,640]{0,1:T(8,128)S(1)}, f32[515,640]{0,1:T(8,128)}, u32[]{:S(2)}) copy-start(f32[515,640]{0,1:T(8,128)} %pad_convert_fusion) | copy-start | bytes 3955204
  110.2 6.1 %copy-start.42 = (f32[640]{0:T(1024)S(1)}, f32[640]{0:T(1024)}, u32[]{:S(2)}) copy-start(f32[640]{0:T(1024)} %get-tuple-element.183) | copy-start | bytes 7684
  110.2 6.1 %copy-start.43 = (f32[640]{0:T(1024)S(1)}, f32[640]{0:T(1024)}, u32[]{:S(2)}) copy-start(f32[640]{0:T(1024)} %get-tuple-element.184) | copy-start | bytes 7684
  110.2 6.1 %copy-start.44 = (f32[640]{0:T(1024)S(1)}, f32[640]{0:T(1024)}, u32[]{:S(2)}) copy-start(f32[640]{0:T(1024)} %get-tuple-element.185) | copy-start | bytes 7684
  116.3 12.8 %copy-start.56 = (bf16[1,2,4]{2,1,0:T(2,128)(2,1)S(1)}, bf16[1,2,4]{2,1,0:T(2,128)(2,1)}, u32[]{:S(2)}) copy-start(bf16[1,2,4]{2,1,0:T(2,128)(2,1)} %convert_element_type.248) | copy-start | bytes 52
  144.2 16.0 %copy-start.31 = (f32[768]{0:T(1024)S(1)}, f32[768]{0:T(1024)}, u32[]{:S(2)}) copy-start(f32[768]{0:T(1024)} %get-tuple-element.178) | copy-start | bytes 9220
  144.2 16.0 %copy-start.32 = (f32[768]{0:T(1024)S(1)}, f32[768]{0:T(1024)}, u32[]{:S(2)}) copy-start(f32[768]{0:T(1024)} %get-tuple-element.179) | copy-start | bytes 9220
  144.2 16.0 %copy-start.33 = (f32[768]{0:T(1024)S(1)}, f32[768]{0:T(1024)}, u32[]{:S(2)}) copy-start(f32[768]{0:T(1024)} %get-tuple-element.180) | copy-start | bytes 9220
  144.2 16.0 %copy-start.34 = (f32[768]{0:T(1024)S(1)}, f32[768]{0:T(1024)}, u32[]{:S(2)}) copy-start(f32[768]{0:T(1024)} %get-tuple-element.181) | copy-start | bytes 9220
  162.1 18.8 %copy-start.20 = (bf16[128,128]{0,1:T(8,128)(2,1)}, bf16[128,128]{0,1:T(8,128)(2,1)S(1)}, u32[]{:S(2)}) copy-start(bf16[128,128]{0,1:T(8,128)(2,1)S(1)} %copy.166) | copy-start | bytes 98308
  181.5 25.4 %copy-start.3 = (f32[2,4,64,64]{3,2,1,0:T(8,128)}, f32[2,4,64,64]{3,2,1,0:T(8,128)S(1)}, u32[]{:S(2)}) copy-start(f32[2,4,64,64]{3,2,1,0:T(8,128)S(1)} %get-tuple-element.175) | copy-start | bytes 393220
  223.3 8.4 %copy-start.4 = (f32[2,4,64,64]{3,2,1,0:T(8,128)S(1)}, f32[2,4,64,64]{3,2,1,0:T(8,128)}, u32[]{:S(2)}) copy-start(f32[2,4,64,64]{3,2,1,0:T(8,128)} %copy-done.3) | copy-start | bytes 393220
  234.5 9.5 %copy-start.7 = (bf16[64,2048]{1,0:T(8,128)(2,1)S(1)}, bf16[64,2048]{1,0:T(8,128)(2,1)}, u32[]{:S(2)}) copy-start(bf16[64,2048]{1,0:T(8,128)(2,1)} %param.22) | copy-start | bytes 786436
  234.9 9.1 %copy-start.30 = (f32[1,2048]{1,0:T(1,128)S(1)}, f32[1,2048]{1,0:T(1,128)}, u32[]{:S(2)}) copy-start(f32[1,2048]{1,0:T(1,128)} %get-tuple-element.226) | copy-start | bytes 24580
  (35 other events, 123.8 us)
where the time goes:
time: 250 us; the launch traced here: 248 us
  blocking collectives  122 us (49%)
  local copies, waits for them, and re-layouts  58.6 us (23%)
  other arithmetic  34.5 us (14%)
  matrix products  28.4 us (11%)
  starting transfers between devices  3.15 us (1%)
    all_gather x4, blocking collectives, prefix(): lax.all_gather(a.astype(kind), axis)  54.2 us
    psum x1, blocking collectives, local(): lax.psum(jnp.dot(own_cols, modulation, preferred_element_type=jnp.float32...  39.4 us
    all_gather x1, blocking collectives, local(): context_cols = lax.all_gather(own_context, 'sp', axis=0, tiled=True)  14.5 us
    dot_general x10, matrix products, project_many(): jnp.dot(row_block, weight, preferred_element_type=jnp.float32)  10.5 us
    all_gather x1, blocking collectives, local(): lax.all_gather(hidden, 'tp', axis=0, tiled=True)  7.17 us
    all_to_all x1, blocking collectives, local(): lax.all_to_all(stacked, 'tp', split_axis=0, concat_axis=2, tiled=True)[0]  6.85 us
    another operation x3, other arithmetic  6.56 us
    exp x4, local copies, waits for them, and re-layouts, directed_pass(): jnp.exp(running)  5.96 us
  transfers between devices with their start and end apart: 2, of which 0 were waited for; matrix products, arithmetic and copies ran while one was open for 28% of the time, Pallas kernels for 0%

commit v1 on v0

v1 whole, which is shorter than its diff:
```python
import functools

import jax
import jax.numpy as jnp
from jax import lax
from jax.experimental import pallas as pl
from jax.experimental.pallas import tpu as pltpu
from jax.sharding import PartitionSpec as P

HEAD_DIM = 64
STATE = 64
HALO = 16
LANES = 128
ROW_EPS = 1e-06
GROUP_EPS = 1e-05
HIGHEST = lax.Precision.HIGHEST
MESH = pl.DeviceIdType.MESH
F32 = jnp.float32
BF16 = jnp.bfloat16


def silu(v):
    return v / (1.0 + jnp.exp(-v))


def softplus(v):
    return jnp.maximum(v, 0.0) + jnp.log1p(jnp.exp(-jnp.abs(v)))


def dot(a, b):
    return jnp.dot(a, b, preferred_element_type=F32)


def dot_nt(a, b):
    return lax.dot_general(a, b, (((1,), (1,)), ((), ())), preferred_element_type=F32)


def dot_tn(a, b):
    return lax.dot_general(a, b, (((0,), (0,)), ((), ())), preferred_element_type=F32)


def split(v):
    hi = v.astype(BF16)
    return hi, (v - hi.astype(F32)).astype(BF16)


def iota(shape, dim):
    return lax.broadcasted_iota(jnp.int32, shape, dim)


def guarded(always, cond, body):
    if always:
        body()
    else:
        pl.when(cond)(body)


def mixer_kernel(
    n_sp, n_tp, reducers,
    cols_h, latent_h, context_h, modulation_h, gain_h, wx_h, wg_h, wb_h, wc_h, wdt_h,
    cx_h, cb_h, cc_h, dec_h, og_h, wout_h,
    out_h,
    cols, mod_w, gain, wx, wg, wb, wc, wdt, cx, cb, cc, dec, og, wout,
    lat, ctx, lat_prev, lat_next, ctx_prev, ctx_next,
    part, part_rx, mod_full, hid_l, hid_c,
    ctx_msg, lat_msg, lat_rx, y_loc, nrm, nrm_rx, out_v,
    in_sem, halo_send, halo_recv, tok_send, tok_recv,
    rs_send, rs_recv, ag_send, ag_recv,
    cm_send, cm_recv, lm_send, lm_recv, nm_send, nm_recv, out_sem,
):
    s = lax.axis_index("sp")
    t = lax.axis_index("tp")
    n = n_sp * n_tp
    rank = s * n_tp + t
    rows = latent_h.shape[0]
    length = lat.shape[0]
    ctx_len = ctx.shape[0]
    width = lat.shape[1]
    head_cols = wx.shape[1]
    state_cols = wb.shape[1]
    heads = head_cols // HEAD_DIM
    groups = state_cols // STATE
    repeat_cols = head_cols // groups
    chunk = part.shape[2]

    barrier = pltpu.get_barrier_semaphore()

    def group_peer(d):
        other = lax.rem(rank + d, n)
        return {"sp": other // n_tp, "tp": lax.rem(other, n_tp)}

    for d in range(1, n):
        pl.semaphore_signal(barrier, inc=1, device_id=group_peer(d), device_id_type=MESH)

    own_rows = pl.ds(pl.multiple_of(t * rows, 16), rows)
    pairs = [
        (cols_h, cols), (modulation_h, mod_w), (latent_h, lat.at[own_rows]), (context_h, ctx),
        (gain_h, gain), (wx_h, wx), (wb_h, wb), (wdt_h, wdt), (cx_h, cx), (cb_h, cb), (dec_h, dec),
        (wc_h, wc), (cc_h, cc), (wg_h, wg), (og_h, og), (wout_h, wout),
    ]
    loads = [pltpu.make_async_copy(a, b, in_sem.at[i]) for i, (a, b) in enumerate(pairs)]
    for c in loads:
        c.start()
    pl.semaphore_wait(barrier, n - 1)

    sends = []

    def remote(src, dst, ssem, rsem, device):
        return pltpu.make_async_remote_copy(
            src_ref=src, dst_ref=dst, send_sem=ssem, recv_sem=rsem,
            device_id=device, device_id_type=MESH,
        )

    after = lax.rem(s + 1, n_sp)
    before = lax.rem(s + n_sp - 1, n_sp)
    tok = []
    for d in range(1, n_tp):
        c = remote(latent_h, lat.at[own_rows], tok_send.at[d], tok_recv.at[d],
                   {"sp": s, "tp": lax.rem(t + d, n_tp)})
        c.start()
        tok.append(c)
    ctx_halo = [
        remote(context_h.at[pl.ds(ctx_len - HALO, HALO)], ctx_prev, halo_send.at[0],
               halo_recv.at[0], {"sp": after, "tp": t}),
        remote(context_h.at[pl.ds(0, HALO)], ctx_next, halo_send.at[1], halo_recv.at[1],
               {"sp": before, "tp": t}),
    ]
    for c in ctx_halo:
        c.start()
    low = [remote(latent_h.at[pl.ds(rows - HALO, HALO)], lat_prev, halo_send.at[4 + u],
                  halo_recv.at[2], {"sp": after, "tp": u}) for u in range(n_tp)]
    high = [remote(latent_h.at[pl.ds(0, HALO)], lat_next, halo_send.at[4 + n_tp + u],
                   halo_recv.at[3], {"sp": before, "tp": u}) for u in range(n_tp)]

    @pl.when(t == n_tp - 1)
    def _():
        for c in low:
            c.start()

    @pl.when(t == 0)
    def _():
        for c in high:
            c.start()

    loads[0].wait()
    loads[1].wait()
    full = reducers == n
    partial = dot(cols[...], mod_w[...])
    for i in range(reducers):
        part[i] = partial[0:2, i * chunk:(i + 1) * chunk]
    rs = []
    for d in range(1, n):
        other = lax.rem(rank + d, n)
        rs.append(remote(part.at[lax.rem(other, reducers)], part_rx.at[d], rs_send.at[d],
                         rs_recv.at[d], group_peer(d)))
        guarded(full, other < reducers, rs[-1].start)

    for i in (2, 3, 4):
        loads[i].wait()
    ag = [remote(mod_full.at[lax.rem(rank, reducers)], mod_full.at[lax.rem(rank, reducers)],
                 ag_send.at[d], ag_recv.at[d], group_peer(d)) for d in range(1, n)]

    def reduce_chunk():
        total = part[lax.rem(rank, reducers)]
        for d in range(1, n):
            rs[d - 1].wait_recv()
            total = total + part_rx[d]
        mod_full[lax.rem(rank, reducers)] = total
        for c in ag:
            c.start()

    guarded(full, rank < reducers, reduce_chunk)

    def normed_rows(halo_prev, halo_next, body):
        edge = jnp.where(
            iota((HALO, width), 0) == 0,
            halo_next[...].astype(F32),
            halo_prev[...].astype(F32),
        )
        values = jnp.concatenate([edge, body[...].astype(F32)], axis=0)
        return values, lax.rsqrt(jnp.mean(values * values, axis=-1, keepdims=True) + ROW_EPS)

    for c in ctx_halo:
        c.wait_recv()
    ctx_vals, ctx_rs = normed_rows(ctx_prev, ctx_next, ctx)
    gain_row = gain[...].astype(F32)

    for d in range(1, n):
        source = lax.rem(rank + n - d, n)
        guarded(full, source < reducers, ag[d - 1].wait_recv)
    mod_rows = jnp.concatenate([mod_full[i] for i in range(reducers)], axis=1)
    shift = mod_rows[:, :width]
    scale = mod_rows[:, width:2 * width]
    gate_row = mod_rows[0:1, 2 * width:]

    def conv(z, taps_ref):
        total_rows = z.shape[0]
        has_prev = jnp.where(s > 0, 1, 0)
        has_next = jnp.where(s < n_sp - 1, 1, 0)
        r = iota(z.shape, 0)
        keep = jnp.where(r == 0, has_next, jnp.where(r < HALO, has_prev, 1))
        z = jnp.where(keep > 0, z, 0.0)
        taps = taps_ref[...].astype(F32)
        u = (
            taps[0:1] * pltpu.roll(z, 2, 0)
            + taps[1:2] * pltpu.roll(z, 1, 0)
            + taps[2:3] * z
            + taps[3:4] * pltpu.roll(z, total_rows - 1, 0)
        )
        return silu(u[HALO:])

    lane_row = iota((1, LANES), 1)
    expander = (
        iota((LANES, 2 * head_cols), 0) == iota((LANES, 2 * head_cols), 1) // HEAD_DIM
    ).astype(F32).astype(BF16)

    def expand(v):
        hi, lo = split(v)
        return dot(hi, expander) + dot(lo, expander)

    def decay_run(log_decay):
        size = log_decay.shape[0]
        i = iota((size, size), 0)
        j = iota((size, size), 1)
        pre = jnp.dot((j <= i).astype(F32), log_decay, precision=HIGHEST,
                      preferred_element_type=F32)
        total = pre[size - 1:size]
        suf = total - pre + log_decay
        return jnp.where(lane_row < heads, pre, suf), total

    def summarize(msg, xs, bm, dt, run, total):
        weight = expand(jnp.exp(total - run) * dt)
        thi, tlo = split(jnp.broadcast_to(total, (16, LANES)))
        tail_hi = dot(thi, expander)
        tail_lo = dot(tlo, expander)
        row = iota((16, repeat_cols), 0)
        for d in range(2):
            base = d * head_cols
            state = dot_tn(bm, (xs * weight[:, base:base + head_cols]).astype(BF16))
            tail = jnp.zeros((16, repeat_cols), F32)
            for g in range(groups):
                lo_c = base + g * repeat_cols
                msg[d, g * STATE:(g + 1) * STATE, :] = state[
                    g * STATE:(g + 1) * STATE, g * repeat_cols:(g + 1) * repeat_cols
                ].astype(BF16)
                tail = jnp.where(row == g, tail_hi[:, lo_c:lo_c + repeat_cols], tail)
                tail = jnp.where(row == groups + g, tail_lo[:, lo_c:lo_c + repeat_cols], tail)
            msg[d, groups * STATE:, :] = tail.astype(BF16)

    hid_c[...] = (
        ctx_vals * ctx_rs * gain_row * (1.0 + scale[1:2]) + shift[1:2]
    ).astype(BF16)
    for i in (5, 6, 7, 8, 9, 10):
        loads[i].wait()
    rate_row = dec[length:length + 1, :]
    ctx_x = conv(dot(hid_c[...], wx[...]), cx)
    ctx_b = conv(dot(hid_c[...], wb[...]), cb).astype(BF16)
    ctx_dt = softplus(dot(hid_c[HALO:, :], wdt[...]))
    ctx_run, ctx_total = decay_run(rate_row * ctx_dt)
    summarize(ctx_msg.at[0], ctx_x, ctx_b, ctx_dt, ctx_run, ctx_total)
    cm = []
    for d in range(1, n_sp):
        c = remote(ctx_msg.at[0], ctx_msg.at[d], cm_send.at[d], cm_recv.at[d],
                   {"sp": lax.rem(s + d, n_sp), "tp": t})
        c.start()
        cm.append(c)

    for c in tok:
        c.wait_recv()
    low[0].wait_recv()
    high[0].wait_recv()
    lat_vals, lat_rs = normed_rows(lat_prev, lat_next, lat)
    hid_l[...] = (
        lat_vals * lat_rs * gain_row * (1.0 + scale[0:1]) + shift[0:1]
    ).astype(BF16)
    lat_x = conv(dot(hid_l[...], wx[...]), cx)
    lat_b = conv(dot(hid_l[...], wb[...]), cb).astype(BF16)
    dt = softplus(dot(hid_l[HALO:, :], wdt[...]))
    run, total = decay_run(rate_row * dt + dec[0:length, :])
    summarize(lat_msg, lat_x, lat_b, dt, run, total)
    lm = []
    for d in range(1, n_sp):
        c = remote(lat_msg.at[(s + d) // n_sp], lat_rx.at[d], lm_send.at[d], lm_recv.at[d],
                   {"sp": lax.rem(s + d, n_sp), "tp": t})
        c.start()
        lm.append(c)

    loads[11].wait()
    loads[12].wait()
    lat_c = conv(dot(hid_l[...], wc[...]), cc).astype(BF16)
    run_t = jnp.transpose(run)
    dt_t = jnp.transpose(dt)
    i_pos = iota((length, length), 0)
    j_pos = iota((length, length), 1)
    lat_xb = lat_x.astype(BF16)
    state_lane = iota((length, state_cols), 1) // STATE
    pair_lane = iota((length, LANES), 1)
    zero_b = jnp.zeros((), BF16)
    per_group = heads // groups
    affinity = [
        dot_nt(jnp.where(state_lane == g, lat_c, zero_b), lat_b) for g in range(groups)
    ]

    def block_weights(h):
        ahead = heads + h
        gap = jnp.where(
            j_pos <= i_pos,
            run[:, h:h + 1] - run_t[h:h + 1, :],
            run[:, ahead:ahead + 1] - run_t[ahead:ahead + 1, :],
        )
        step = jnp.where(j_pos <= i_pos, dt_t[h:h + 1, :], 0.0) + jnp.where(
            j_pos >= i_pos, dt_t[ahead:ahead + 1, :], 0.0
        )
        return (affinity[h // per_group] * jnp.exp(gap) * step).astype(BF16)

    for q in range(heads // 2):
        both = lat_xb[:, q * LANES:(q + 1) * LANES]
        y_loc[:, q * LANES:(q + 1) * LANES] = dot(
            jnp.concatenate([block_weights(2 * q), block_weights(2 * q + 1)], axis=1),
            jnp.concatenate(
                [
                    jnp.where(pair_lane < HEAD_DIM, both, zero_b),
                    jnp.where(pair_lane >= HEAD_DIM, both, zero_b),
                ],
                axis=0,
            ),
        )
    reach = expand(jnp.exp(run))
    loads[13].wait()
    loads[14].wait()
    gate_act = silu(dot(hid_l[HALO:, :], wg[...]))

    def totals(tail):
        rows16 = tail.astype(F32)
        return [rows16[g:g + 1] + rows16[groups + g:groups + g + 1] for g in range(groups)]

    srows = [pl.ds(g * STATE, STATE) for g in range(groups)]
    trows = pl.ds(groups * STATE, 16)
    for c in cm:
        c.wait_recv()
    start = []
    for d in range(2):
        acc = [jnp.zeros((1, repeat_cols), F32) for _ in range(groups)]
        state = [jnp.zeros((STATE, repeat_cols), F32) for _ in range(groups)]
        for k in range(n_sp):
            place = n_sp - 1 - k if d == 0 else k
            slot = lax.rem(s + n_sp - place, n_sp)
            tot = totals(ctx_msg[slot, d, trows, :])
            for g in range(groups):
                state[g] = state[g] + jnp.exp(acc[g]) * ctx_msg[slot, d, srows[g], :].astype(F32)
                acc[g] = acc[g] + tot[g]
        start.append(state)
    for c in lm:
        c.wait_recv()
    mixed_y = y_loc[...]
    for d in range(2):
        acc = [jnp.zeros((1, repeat_cols), F32) for _ in range(groups)]
        state = [jnp.zeros((STATE, repeat_cols), F32) for _ in range(groups)]
        for e in range(1, n_sp):
            slot = e if d == 0 else n_sp - e
            valid = (s >= e) if d == 0 else (s + e < n_sp)
            live = jnp.where(valid, 1.0, 0.0)
            tot = totals(lat_rx[slot, trows, :])
            for g in range(groups):
                state[g] = state[g] + live * (
                    jnp.exp(acc[g]) * lat_rx[slot, srows[g], :].astype(F32)
                )
                acc[g] = acc[g] + live * tot[g]
        blocks = []
        for g in range(groups):
            entry = (state[g] + jnp.exp(acc[g]) * start[d][g]).astype(BF16)
            pieces = [
                entry if k == g else jnp.zeros((STATE, repeat_cols), BF16) for k in range(groups)
            ]
            blocks.append(jnp.concatenate(pieces, axis=1) if groups > 1 else entry)
        entry_all = jnp.concatenate(blocks, axis=0) if groups > 1 else blocks[0]
        mixed_y = mixed_y + reach[:, d * head_cols:(d + 1) * head_cols] * dot(lat_c, entry_all)
    gated = mixed_y * gate_act
    og_row = og[...].astype(F32)
    for g in range(groups):
        part_g = gated[:, g * repeat_cols:(g + 1) * repeat_cols]
        ms = jnp.mean(part_g * part_g, axis=-1, keepdims=True)
        nrm[:, g * repeat_cols:(g + 1) * repeat_cols] = (
            part_g * lax.rsqrt(ms + GROUP_EPS) * og_row[:, g * repeat_cols:(g + 1) * repeat_cols]
        ).astype(BF16)

    nm = []
    for d in range(1, n_tp):
        u = lax.rem(t + d, n_tp)
        c = remote(nrm.at[pl.ds(pl.multiple_of(u * rows, 16), rows)], nrm_rx.at[d],
                   nm_send.at[d], nm_recv.at[d], {"sp": s, "tp": u})
        c.start()
        nm.append(c)
    loads[15].wait()

    def out_rows(u):
        return wout[pl.ds(pl.multiple_of(u * head_cols, 16), head_cols), :]

    branch = dot(nrm[own_rows, :], out_rows(t))
    for d in range(1, n_tp):
        nm[d - 1].wait_recv()
        branch = branch + dot(nrm_rx[d], out_rows(lax.rem(t + n_tp - d, n_tp)))
    out_v[...] = (lat[own_rows, :].astype(F32) + gate_row * branch).astype(BF16)
    final = pltpu.make_async_copy(out_v, out_h, out_sem)
    final.start()

    for c in tok + ctx_halo + cm + lm + nm:
        c.wait_send()

    @pl.when(t == n_tp - 1)
    def _():
        for c in low:
            c.wait_send()

    @pl.when(t == 0)
    def _():
        for c in high:
            c.wait_send()

    for d in range(1, n):
        other = lax.rem(rank + d, n)
        guarded(full, other < reducers, rs[d - 1].wait_send)

    def ag_done():
        for c in ag:
            c.wait_send()

    guarded(full, rank < reducers, ag_done)
    final.wait()


def local(
    latent, cond, context, context_cond, modulation, norm_gain, w_x, w_gate, w_b, w_c, w_dt,
    conv_x, conv_b, conv_c, decay_rate, decay_extra, out_gain, w_out,
):
    n_sp = lax.axis_size("sp")
    n_tp = lax.axis_size("tp")
    n = n_sp * n_tp
    rows, width = latent.shape
    length = decay_extra.shape[0]
    ctx_len = context.shape[0]
    share = modulation.shape[0]
    mod_cols = modulation.shape[1]
    head_cols = w_x.shape[1]
    state_cols = w_b.shape[1]
    heads = w_dt.shape[2]
    groups = state_cols // STATE
    repeat_cols = head_cols // groups
    reducers = max(m for m in range(1, n + 1) if mod_cols % (LANES * m) == 0)
    chunk = mod_cols // reducers

    cond_rows = silu(jnp.stack([cond, context_cond]).astype(F32)).astype(BF16)
    own_cols = lax.dynamic_slice_in_dim(
        cond_rows, lax.axis_index(("sp", "tp")) * share, share, 1
    )
    cols = jnp.pad(own_cols, ((0, 14), (0, 0)))
    wdt = jnp.pad(
        jnp.concatenate([w_dt[0], w_dt[1]], axis=1), ((0, 0), (0, LANES - 2 * heads))
    )
    dec = jnp.pad(
        jnp.concatenate(
            [
                jnp.concatenate([decay_extra, decay_extra], axis=1),
                jnp.broadcast_to(-decay_rate.reshape(1, 2 * heads), (8, 2 * heads)),
            ],
            axis=0,
        ),
        ((0, 0), (0, LANES - 2 * heads)),
    )
    args = (
        cols, latent, context, modulation, norm_gain.reshape(1, width), w_x, w_gate, w_b, w_c,
        wdt, conv_x, conv_b, conv_c, dec, out_gain.reshape(1, head_cols), w_out,
    )
    V = pltpu.VMEM
    D = pltpu.SemaphoreType.DMA
    held = [args[i] for i in (0, 3, 4, 5, 6, 7, 8, 9, 10, 11, 12, 13, 14, 15)]
    msg = (groups * STATE + 16, repeat_cols)
    scratch = [V(a.shape, a.dtype) for a in held] + [
        V((length, width), BF16),
        V((ctx_len, width), BF16),
        V((HALO, width), BF16),
        V((HALO, width), BF16),
        V((HALO, width), BF16),
        V((HALO, width), BF16),
        V((reducers, 2, chunk), F32),
        V((n, 2, chunk), F32),
        V((reducers, 2, chunk), F32),
        V((length + HALO, width), BF16),
        V((ctx_len + HALO, width), BF16),
        V((n_sp, 2) + msg, BF16),
        V((2,) + msg, BF16),
        V((n_sp,) + msg, BF16),
        V((length, head_cols), F32),
        V((length, head_cols), BF16),
        V((n_tp, rows, head_cols), BF16),
        V((rows, width), BF16),
        D((len(args),)),
        D((4 + 2 * n_tp,)),
        D((4,)),
        D((n_tp,)), D((n_tp,)),
        D((n,)), D((n,)), D((n,)), D((n,)),
        D((n_sp,)), D((n_sp,)), D((n_sp,)), D((n_sp,)),
        D((n_tp,)), D((n_tp,)),
        D,
    ]
    return pl.pallas_call(
        functools.partial(mixer_kernel, n_sp, n_tp, reducers),
        out_shape=jax.ShapeDtypeStruct((rows, width), BF16),
        in_specs=[pl.BlockSpec(memory_space=pl.ANY)] * len(args),
        out_specs=pl.BlockSpec(memory_space=pl.ANY),
        scratch_shapes=scratch,
        compiler_params=pltpu.CompilerParams(
            collective_id=0, has_side_effects=True, vmem_limit_bytes=60 * 1024 * 1024
        ),
    )(*args)


def solution(mesh):
    in_specs = (
        P(("dp", "sp", "tp"), None),
        P("dp"),
        P(("dp", "sp"), None),
        P(),
        P(("sp", "tp"), None),
        P(),
        P(None, "tp"),
        P(None, "tp"),
        P(None, "tp"),
        P(None, "tp"),
        P(None, None, "tp"),
        P(None, "tp"),
        P(None, "tp"),
        P(None, "tp"),
        P(None, "tp"),
        P(("dp", "sp"), "tp"),
        P("tp"),
        P(),
    )
    out_specs = P(("dp", "sp", "tp"), None)
    return jax.shard_map(local, mesh=mesh, in_specs=in_specs, out_specs=out_specs, check_vma=False)
```

time: 250 us -> 55.9 us (0.22)
  blocking collectives: 122 us -> 0 us
  local copies, waits for them, and re-layouts: 58.6 us -> 9.05 us
  Pallas kernels: 0 us -> 44.9 us
  other arithmetic: 34.5 us -> 1.54 us
  matrix products: 28.4 us -> 0 us
  starting transfers between devices: 3.15 us -> 0 us
    all_gather x6 -> x0, blocking collectives: 75.8 us -> none  [the longest x4 54.2 us: prefix(): lax.all_gather(a.astype(kind), axis)]
    pallas_call x0 -> x1, Pallas kernels: none -> 44.9 us  [local(): pl.pallas_call(functools.partial(mixer_kernel, n_sp, n_tp, reducers), out...]
    psum x1 -> x0, blocking collectives: 39.4 us -> none  [local(): lax.psum(jnp.dot(own_cols, modulation, preferred_element_type=jnp.float32...]
    dot_general x24 -> x0, matrix products: 28.4 us -> none  [the longest x10 10.5 us: project_many(): jnp.dot(row_block, weight, preferred_element_type=jnp.float32)]
    exp x8 -> x0, local copies, waits for them, and re-layouts: 11.6 us -> none  [the longest x4 5.96 us: directed_pass(): jnp.exp(running)]
    another operation x8 -> x0, other arithmetic: 11 us -> none
    rev x10 -> x0, local copies, waits for them, and re-layouts: 10.4 us -> none  [the longest x2 2.97 us: local(): latent_xs[::-1]]
    mul x6 -> x0, local copies, waits for them, and re-layouts: 7.25 us -> none  [the longest x2 2.55 us: advance(): to_end = jnp.exp(running[-1:] - running) * step_blk]
  transfers between devices with their start and end apart: 2 -> 0, of which waited for: 0 -> 0; matrix products, arithmetic and copies ran while one was open for 28% -> 0% of each run, Pallas kernels for 0% -> 0%
where the time goes in v1:
time: 55.9 us; the launch traced here: 55.5 us
  Pallas kernels  44.9 us (80%)
  local copies, waits for them, and re-layouts  9.05 us (16%)
  other arithmetic  1.54 us (3%)
    pallas_call x1, Pallas kernels, local(): pl.pallas_call(functools.partial(mixer_kernel, n_sp, n_tp, reducers), out...  44.9 us
    unnamed x1, local copies, waits for them, and re-layouts  1.67 us
    another operation x2, local copies, waits for them, and re-layouts, local(): cond_rows = silu(jnp.stack([cond, context_cond]).astype(F32)).astype(BF16)  1.39 us
    reshape x1, local copies, waits for them, and re-layouts, local(): norm_gain.reshape(1, width)  1.29 us
    reshape x1, local copies, waits for them, and re-layouts, local(): out_gain.reshape(1, head_cols)  1.25 us

profile of v1, /device:TPU:0, one launch (start us, length us, event | category | flops | bytes accessed | tf_op | source)
XLA Modules:
  0.0 55.5 jit_solution(3970598393451271911)
XLA Ops:
  0.0 0.7 %stack.10 = bf16[1,2048]{1,0:T(2,128)(2,1)S(1)} reshape(bf16[2048]{0:T(1024)(128)(2,1)} %param.21) | data formatting | bytes 8192 | tf_op jit(solution)/shard_map/stack | solution.py:452
  0.7 0.7 %stack.9 = bf16[1,2048]{1,0:T(2,128)(2,1)S(1)} reshape(bf16[2048]{0:T(1024)(128)(2,1)} %param.19) | data formatting | bytes 8192 | tf_op jit(solution)/shard_map/stack | solution.py:452
  1.4 0.1 fusion.2
  1.5 0.6 %pad.12.cols_h = bf16[16,256]{1,0:T(8,128)(2,1)} pad(bf16[2,256]{1,0:T(2,128)(2,1)S(1)} %fusion.2, bf16[]{:T(256)} %constant.22.clone.1), padding=0_14x0_0 | pad | bytes 9218 | tf_op jit(solution)/shard_map/jit(_pad)/pad | solution.py:456
  2.1 0.8 %slice_bitcast_fusion.1 = (bf16[2048,8]{0,1:T(8,128)(2,1)S(1)}, bf16[2048,8]{0,1:T(8,128)(2,1)S(1)}) fusion(bf16[2,2048,8]{1,2,0:T(8,128)(2,1)} %param.28), kind=kLoop, calls=%fused_computation.2 | loop fusion | bytes 131072 | tf_op jit(solution)/shard_map/squeeze | solution.py:458
  2.9 0.3 copy.23
  3.2 0.9 %pad.13.wdt_h = bf16[2048,128]{1,0:T(8,128)(2,1)} pad(bf16[2048,16]{1,0:T(8,128)(2,1)S(1)} %copy.23, bf16[]{:T(256)} %constant.22.clone.1), padding=0_0x0_112 | pad | bytes 589826 | tf_op jit(solution)/shard_map/jit(_pad)/pad | solution.py:457
  4.0 0.7 %neg.15 = f32[2,8]{1,0:T(2,128)S(1)} negate(f32[2,8]{1,0:T(2,128)} %param.32) | non-fusion elementwise | flops 16 | bytes 128 | tf_op jit(solution)/shard_map/neg | solution.py:464
  4.7 0.1 neg.16
  4.8 0.1 broadcast_in_dim.2
  4.9 0.8 %pad_maximum_fusion.1 = f32[136,16]{0,1:T(8,128)S(1)} fusion(f32[8,16]{0,1:T(8,128)S(1)} %broadcast_in_dim.2, f32[128,8]{0,1:T(8,128)} %param.33), kind=kLoop, calls=%fused_computation.3 | loop fusion | flops 4352 | bytes 13312 | tf_op jit(solution)/shard_map/concatenate | solution.py:461
  5.7 0.1 copy.24
  5.8 0.6 %pad.14.dec_h = f32[136,128]{1,0:T(8,128)} pad(f32[136,16]{1,0:T(8,128)S(1)} %copy.24, f32[]{:T(128)} %constant.23.clone.1), padding=0_0x0_112 | pad | bytes 78340 | tf_op jit(solution)/shard_map/jit(_pad)/pad | solution.py:460
  6.4 1.3 %reshape.15.gain_h = bf16[1,2048]{1,0:T(2,128)(2,1)} reshape(bf16[2048]{0:T(1024)(128)(2,1)} %param.23) | data formatting | bytes 8192 | tf_op jit(solution)/shard_map/reshape | solution.py:471
  7.7 1.3 %reshape.16.og_h = bf16[1,512]{1,0:T(2,128)(2,1)} reshape(bf16[512]{0:T(512)(128)(2,1)} %param.34) | data formatting | bytes 2048 | tf_op jit(solution)/shard_map/reshape | solution.py:472
  8.9 44.9 %shard_map.172 = bf16[64,2048]{1,0:T(8,128)(2,1)} custom-call(bf16[16,256]{1,0:T(8,128)(2,1)} %pad.12.cols_h, bf16[64,2048]{1,0:T(8,128)(2,1)} %latent_h.1, bf16[128,2048]{1,0:T(8,128)(2,1)} %context_h.1, bf16[256,6144]{1,0:T(8,128)(2,1)} %modulation_h.1, bf16[1,2048]{1,0:T(2,128)(2,1)} %reshape.15.gain_h, bf16[2048,512]{1,0:T(8,128)(2,1)} %wx_h.1, ...), custom_call_target="tpu_custom_call" | custom-call | tf_op jit(solution)/shard_map/pallas_call | solution.py:506
  53.9 1.7 %copy.26 = bf16[64,2048]{1,0:T(8,128)(2,1)} copy(bf16[64,2048]{1,0:T(8,128)(2,1)} %shard_map.172) | data formatting | bytes 524288
  (1 shorter events, 0.0 us)

commit v2 on v1

--- a/solution.py
+++ b/solution.py
@@ -48,6 +48,22 @@
     return lax.broadcasted_iota(jnp.int32, shape, dim)
 
 
+def flat_row(tiled):
+    return jnp.concatenate([tiled[i:i + 1] for i in range(tiled.shape[0])], axis=1)
+
+
+def own_cond(rows_ref, k, rank, share):
+    if share % LANES == 0:
+        count = share // LANES
+        return jnp.concatenate(
+            [rows_ref[k, pl.ds(rank * count + i, 1), :] for i in range(count)], axis=1
+        )
+    per = LANES // share
+    row = jnp.broadcast_to(rows_ref[k, pl.ds(rank // per, 1), :], (8, LANES))
+    moved = pltpu.roll(row, lax.rem(LANES - lax.rem(rank, per) * share, LANES), 1)
+    return moved[0:1, :share]
+
+
 def guarded(always, cond, body):
     if always:
         body()
@@ -57,10 +73,11 @@
 
 def mixer_kernel(
     n_sp, n_tp, reducers,
-    cols_h, latent_h, context_h, modulation_h, gain_h, wx_h, wg_h, wb_h, wc_h, wdt_h,
-    cx_h, cb_h, cc_h, dec_h, og_h, wout_h,
+    cond_h, latent_h, context_h, modulation_h, gain_h, wx_h, wg_h, wb_h, wc_h, wdt_h,
+    cx_h, cb_h, cc_h, extra_h, og_h, wout_h, ccond_h, rate_h,
     out_h,
-    cols, mod_w, gain, wx, wg, wb, wc, wdt, cx, cb, cc, dec, og, wout,
+    cond, mod_w, gain, wx, wg, wb, wc, wdt, cx, cb, cc, extra, og, wout, ccond, rate,
+    cond_rows, wdt_all,
     lat, ctx, lat_prev, lat_next, ctx_prev, ctx_next,
     part, part_rx, mod_full, hid_l, hid_c,
     ctx_msg, lat_msg, lat_rx, y_loc, nrm, nrm_rx, out_v,
@@ -94,9 +111,10 @@
 
     own_rows = pl.ds(pl.multiple_of(t * rows, 16), rows)
     pairs = [
-        (cols_h, cols), (modulation_h, mod_w), (latent_h, lat.at[own_rows]), (context_h, ctx),
-        (gain_h, gain), (wx_h, wx), (wb_h, wb), (wdt_h, wdt), (cx_h, cx), (cb_h, cb), (dec_h, dec),
-        (wc_h, wc), (cc_h, cc), (wg_h, wg), (og_h, og), (wout_h, wout),
+        (cond_h, cond), (modulation_h, mod_w), (latent_h, lat.at[own_rows]), (context_h, ctx),
+        (gain_h, gain), (wx_h, wx), (wb_h, wb), (wdt_h, wdt), (cx_h, cx), (cb_h, cb),
+        (extra_h, extra), (wc_h, wc), (cc_h, cc), (wg_h, wg), (og_h, og), (wout_h, wout),
+        (ccond_h, ccond), (rate_h, rate),
     ]
     loads = [pltpu.make_async_copy(a, b, in_sem.at[i]) for i, (a, b) in enumerate(pairs)]
     for c in loads:
@@ -143,9 +161,15 @@
             c.start()
 
     loads[0].wait()
+    loads[16].wait()
+    cond_rows[0] = silu(cond[...].astype(F32))
+    cond_rows[1] = silu(ccond[...].astype(F32))
+    own = [own_cond(cond_rows, k, rank, mod_w.shape[0]) for k in range(2)]
+    pick = iota((16, mod_w.shape[0]), 0)
+    cols = jnp.where(pick == 0, own[0], jnp.where(pick == 1, own[1], 0.0)).astype(BF16)
     loads[1].wait()
     full = reducers == n
-    partial = dot(cols[...], mod_w[...])
+    partial = dot(cols, mod_w[...])
     for i in range(reducers):
         part[i] = partial[0:2, i * chunk:(i + 1) * chunk]
     rs = []
@@ -183,7 +207,17 @@
     for c in ctx_halo:
         c.wait_recv()
     ctx_vals, ctx_rs = normed_rows(ctx_prev, ctx_next, ctx)
-    gain_row = gain[...].astype(F32)
+    gain_row = flat_row(gain[...].astype(F32))
+    for i in (7, 10, 17):
+        loads[i].wait()
+    spare = LANES - 2 * heads
+    wdt_all[...] = jnp.concatenate(
+        [wdt[0].astype(F32), wdt[1].astype(F32), jnp.zeros((spare, width), F32)], axis=0
+    ).astype(BF16)
+    extra_all = jnp.transpose(
+        jnp.concatenate([extra[...], extra[...], jnp.zeros((spare, length), F32)], axis=0)
+    )
+    rate_row = -jnp.concatenate([rate[0:1, :], rate[1:2, :], jnp.zeros((1, spare), F32)], axis=1)
 
     for d in range(1, n):
         source = lax.rem(rank + n - d, n)
@@ -250,12 +284,11 @@
     hid_c[...] = (
         ctx_vals * ctx_rs * gain_row * (1.0 + scale[1:2]) + shift[1:2]
     ).astype(BF16)
-    for i in (5, 6, 7, 8, 9, 10):
+    for i in (5, 6, 8, 9):
         loads[i].wait()
-    rate_row = dec[length:length + 1, :]
     ctx_x = conv(dot(hid_c[...], wx[...]), cx)
     ctx_b = conv(dot(hid_c[...], wb[...]), cb).astype(BF16)
-    ctx_dt = softplus(dot(hid_c[HALO:, :], wdt[...]))
+    ctx_dt = softplus(dot_nt(hid_c[HALO:, :], wdt_all[...]))
     ctx_run, ctx_total = decay_run(rate_row * ctx_dt)
     summarize(ctx_msg.at[0], ctx_x, ctx_b, ctx_dt, ctx_run, ctx_total)
     cm = []
@@ -275,8 +308,8 @@
     ).astype(BF16)
     lat_x = conv(dot(hid_l[...], wx[...]), cx)
     lat_b = conv(dot(hid_l[...], wb[...]), cb).astype(BF16)
-    dt = softplus(dot(hid_l[HALO:, :], wdt[...]))
-    run, total = decay_run(rate_row * dt + dec[0:length, :])
+    dt = softplus(dot_nt(hid_l[HALO:, :], wdt_all[...]))
+    run, total = decay_run(rate_row * dt + extra_all)
     summarize(lat_msg, lat_x, lat_b, dt, run, total)
     lm = []
     for d in range(1, n_sp):
@@ -376,7 +409,7 @@
         entry_all = jnp.concatenate(blocks, axis=0) if groups > 1 else blocks[0]
         mixed_y = mixed_y + reach[:, d * head_cols:(d + 1) * head_cols] * dot(lat_c, entry_all)
     gated = mixed_y * gate_act
-    og_row = og[...].astype(F32)
+    og_row = flat_row(og[...].astype(F32))
     for g in range(groups):
         part_g = gated[:, g * repeat_cols:(g + 1) * repeat_cols]
         ms = jnp.mean(part_g * part_g, axis=-1, keepdims=True)
@@ -439,43 +472,27 @@
     rows, width = latent.shape
     length = decay_extra.shape[0]
     ctx_len = context.shape[0]
-    share = modulation.shape[0]
     mod_cols = modulation.shape[1]
     head_cols = w_x.shape[1]
     state_cols = w_b.shape[1]
-    heads = w_dt.shape[2]
     groups = state_cols // STATE
     repeat_cols = head_cols // groups
     reducers = max(m for m in range(1, n + 1) if mod_cols % (LANES * m) == 0)
     chunk = mod_cols // reducers
 
-    cond_rows = silu(jnp.stack([cond, context_cond]).astype(F32)).astype(BF16)
-    own_cols = lax.dynamic_slice_in_dim(
-        cond_rows, lax.axis_index(("sp", "tp")) * share, share, 1
-    )
-    cols = jnp.pad(own_cols, ((0, 14), (0, 0)))
-    wdt = jnp.pad(
-        jnp.concatenate([w_dt[0], w_dt[1]], axis=1), ((0, 0), (0, LANES - 2 * heads))
-    )
-    dec = jnp.pad(
-        jnp.concatenate(
-            [
-                jnp.concatenate([decay_extra, decay_extra], axis=1),
-                jnp.broadcast_to(-decay_rate.reshape(1, 2 * heads), (8, 2 * heads)),
-            ],
-            axis=0,
-        ),
-        ((0, 0), (0, LANES - 2 * heads)),
-    )
     args = (
-        cols, latent, context, modulation, norm_gain.reshape(1, width), w_x, w_gate, w_b, w_c,
-        wdt, conv_x, conv_b, conv_c, dec, out_gain.reshape(1, head_cols), w_out,
+        cond.reshape(-1, LANES), latent, context, modulation, norm_gain.reshape(-1, LANES),
+        w_x, w_gate, w_b, w_c, jnp.swapaxes(w_dt, 1, 2), conv_x, conv_b, conv_c,
+        decay_extra.T, out_gain.reshape(-1, LANES), w_out, context_cond.reshape(-1, LANES),
+        decay_rate,
     )
     V = pltpu.VMEM
     D = pltpu.SemaphoreType.DMA
-    held = [args[i] for i in (0, 3, 4, 5, 6, 7, 8, 9, 10, 11, 12, 13, 14, 15)]
+    held = [args[i] for i in (0, 3, 4, 5, 6, 7, 8, 9, 10, 11, 12, 13, 14, 15, 16, 17)]
     msg = (groups * STATE + 16, repeat_cols)
     scratch = [V(a.shape, a.dtype) for a in held] + [
+        V((2, width // LANES, LANES), F32),
+        V((LANES, width), BF16),
         V((length, width), BF16),
         V((ctx_len, width), BF16),
         V((HALO, width), BF16),

time: 55.9 us -> 47 us (0.84)
  local copies, waits for them, and re-layouts: 9.05 us -> 1.67 us
  other arithmetic: 1.54 us -> 0 us
    reshape x2 -> x0, local copies, waits for them, and re-layouts: 2.54 us -> none  [the longest x1 1.29 us: local(): norm_gain.reshape(1, width)]
    pad x3 -> x0, local copies, waits for them, and re-layouts: 2.14 us -> none  [the longest x1 0.89 us: local(): jnp.pad(jnp.concatenate([w_dt[0], w_dt[1]], axis=1), ((0, 0), (0, LANES -...]
    another operation x2 -> x0, local copies, waits for them, and re-layouts: 1.39 us -> none  [local(): cond_rows = silu(jnp.stack([cond, context_cond]).astype(F32)).astype(BF16)]
    squeeze x1 -> x0, local copies, waits for them, and re-layouts: 0.78 us -> none  [local(): w_dt[0]]
    concatenate x2 -> x0, other arithmetic: 0.77 us -> none  [the longest x1 0.77 us: local(): jnp.concatenate([jnp.concatenate([decay_extra, decay_extra], axis=1), jnp...]
    neg x1 -> x0, other arithmetic: 0.68 us -> none  [local(): -decay_rate.reshape(1, 2 * heads)]
where the time goes in v2:
time: 47 us; the launch traced here: 46.8 us
  Pallas kernels  45.2 us (96%)
  local copies, waits for them, and re-layouts  1.67 us (4%)
    pallas_call x1, Pallas kernels, local(): pl.pallas_call(functools.partial(mixer_kernel, n_sp, n_tp, reducers), out...  45.2 us
    unnamed x1, local copies, waits for them, and re-layouts  1.67 us

profile of v2, /device:TPU:0, one launch (start us, length us, event | category | flops | bytes accessed | tf_op | source)
XLA Modules:
  0.0 46.8 jit_solution(2595555174344759854)
XLA Ops:
  0.0 45.2 %shard_map.172 = bf16[64,2048]{1,0:T(8,128)(2,1)} custom-call(bf16[16,128]{1,0:T(8,128)(2,1)} %bitcast.7, bf16[64,2048]{1,0:T(8,128)(2,1)} %latent_h.1, bf16[128,2048]{1,0:T(8,128)(2,1)} %context_h.1, bf16[256,6144]{1,0:T(8,128)(2,1)} %modulation_h.1, bf16[16,128]{1,0:T(8,128)(2,1)} %bitcast.8, bf16[2048,512]{1,0:T(8,128)(2,1)} %wx_h.1, ...), custom_call_target="tpu_custom_call" | custom-call | tf_op jit(solution)/shard_map/pallas_call | solution.py:523
  45.2 1.7 %copy.20 = bf16[64,2048]{1,0:T(8,128)(2,1)} copy(bf16[64,2048]{1,0:T(8,128)(2,1)} %shard_map.172) | data formatting | bytes 524288

commit v3 on v2

--- a/solution.py
+++ b/solution.py
@@ -80,10 +80,10 @@
     cond_rows, wdt_all,
     lat, ctx, lat_prev, lat_next, ctx_prev, ctx_next,
     part, part_rx, mod_full, hid_l, hid_c,
-    ctx_msg, lat_msg, lat_rx, y_loc, nrm, nrm_rx, out_v,
+    ctx_st, lat_st, ent_tx, ent_rx, y_loc, nrm, nrm_rx, out_v,
     in_sem, halo_send, halo_recv, tok_send, tok_recv,
     rs_send, rs_recv, ag_send, ag_recv,
-    cm_send, cm_recv, lm_send, lm_recv, nm_send, nm_recv, out_sem,
+    cm_send, cm_recv, lm_send, lm_recv, em_send, em_recv, nm_send, nm_recv, out_sem,
 ):
     s = lax.axis_index("sp")
     t = lax.axis_index("tp")
@@ -262,24 +262,33 @@
         suf = total - pre + log_decay
         return jnp.where(lane_row < heads, pre, suf), total
 
-    def summarize(msg, xs, bm, dt, run, total):
+    blocks = [(d, g, (d * groups + g) % n_sp) for d in range(2) for g in range(groups)]
+
+    def summarize(held, xs, bm, dt, run, total):
         weight = expand(jnp.exp(total - run) * dt)
         thi, tlo = split(jnp.broadcast_to(total, (16, LANES)))
-        tail_hi = dot(thi, expander)
-        tail_lo = dot(tlo, expander)
-        row = iota((16, repeat_cols), 0)
-        for d in range(2):
-            base = d * head_cols
-            state = dot_tn(bm, (xs * weight[:, base:base + head_cols]).astype(BF16))
-            tail = jnp.zeros((16, repeat_cols), F32)
-            for g in range(groups):
-                lo_c = base + g * repeat_cols
-                msg[d, g * STATE:(g + 1) * STATE, :] = state[
-                    g * STATE:(g + 1) * STATE, g * repeat_cols:(g + 1) * repeat_cols
-                ].astype(BF16)
-                tail = jnp.where(row == g, tail_hi[:, lo_c:lo_c + repeat_cols], tail)
-                tail = jnp.where(row == groups + g, tail_lo[:, lo_c:lo_c + repeat_cols], tail)
-            msg[d, groups * STATE:, :] = tail.astype(BF16)
+        tail = jnp.where(
+            iota((16, 2 * head_cols), 0) == 0, dot(thi, expander), dot(tlo, expander)
+        ).astype(BF16)
+        states = [
+            dot_tn(bm, (xs * weight[:, d * head_cols:(d + 1) * head_cols]).astype(BF16))
+            for d in range(2)
+        ]
+        for b, (d, g, _) in enumerate(blocks):
+            lo = g * repeat_cols
+            held[b, s, 0:STATE, :] = states[d][
+                g * STATE:(g + 1) * STATE, lo:lo + repeat_cols
+            ].astype(BF16)
+            lo = d * head_cols + lo
+            held[b, s, STATE:, :] = tail[:, lo:lo + repeat_cols]
+
+    def to_owner(held, b, source, ssem, rsem):
+        return remote(held.at[b, source], held.at[b, source], ssem.at[b],
+                      rsem.at[b * n_sp + source], {"sp": blocks[b][2], "tp": t})
+
+    def send_blocks(held, ssem, rsem):
+        for b, (_, _, owner) in enumerate(blocks):
+            pl.when(s != owner)(to_owner(held, b, s, ssem, rsem).start)
 
     hid_c[...] = (
         ctx_vals * ctx_rs * gain_row * (1.0 + scale[1:2]) + shift[1:2]
@@ -290,13 +299,8 @@
     ctx_b = conv(dot(hid_c[...], wb[...]), cb).astype(BF16)
     ctx_dt = softplus(dot_nt(hid_c[HALO:, :], wdt_all[...]))
     ctx_run, ctx_total = decay_run(rate_row * ctx_dt)
-    summarize(ctx_msg.at[0], ctx_x, ctx_b, ctx_dt, ctx_run, ctx_total)
-    cm = []
-    for d in range(1, n_sp):
-        c = remote(ctx_msg.at[0], ctx_msg.at[d], cm_send.at[d], cm_recv.at[d],
-                   {"sp": lax.rem(s + d, n_sp), "tp": t})
-        c.start()
-        cm.append(c)
+    summarize(ctx_st, ctx_x, ctx_b, ctx_dt, ctx_run, ctx_total)
+    send_blocks(ctx_st, cm_send, cm_recv)
 
     for c in tok:
         c.wait_recv()
@@ -310,13 +314,8 @@
     lat_b = conv(dot(hid_l[...], wb[...]), cb).astype(BF16)
     dt = softplus(dot_nt(hid_l[HALO:, :], wdt_all[...]))
     run, total = decay_run(rate_row * dt + extra_all)
-    summarize(lat_msg, lat_x, lat_b, dt, run, total)
-    lm = []
-    for d in range(1, n_sp):
-        c = remote(lat_msg.at[(s + d) // n_sp], lat_rx.at[d], lm_send.at[d], lm_recv.at[d],
-                   {"sp": lax.rem(s + d, n_sp), "tp": t})
-        c.start()
-        lm.append(c)
+    summarize(lat_st, lat_x, lat_b, dt, run, total)
+    send_blocks(lat_st, lm_send, lm_recv)
 
     loads[11].wait()
     loads[12].wait()
@@ -363,50 +362,51 @@
     loads[14].wait()
     gate_act = silu(dot(hid_l[HALO:, :], wg[...]))
 
-    def totals(tail):
-        rows16 = tail.astype(F32)
-        return [rows16[g:g + 1] + rows16[groups + g:groups + g + 1] for g in range(groups)]
-
-    srows = [pl.ds(g * STATE, STATE) for g in range(groups)]
-    trows = pl.ds(groups * STATE, 16)
-    for c in cm:
-        c.wait_recv()
-    start = []
+    def entry_copy(b, k):
+        return remote(ent_tx.at[b, k], ent_rx.at[b], em_send.at[b * n_sp + k], em_recv.at[b],
+                      {"sp": k, "tp": t})
+
+    def growth(held, b, k):
+        tail = held[b, k, STATE:, :].astype(F32)
+        return jnp.exp(tail[0:1] + tail[1:2])
+
+    def scan_block(b, d, owner):
+        order = list(range(n_sp)) if d == 0 else list(range(n_sp - 1, -1, -1))
+        for k in range(n_sp):
+            if k != owner:
+                to_owner(ctx_st, b, k, cm_send, cm_recv).wait_recv()
+        state = jnp.zeros((STATE, repeat_cols), F32)
+        for k in order:
+            state = growth(ctx_st, b, k) * state + ctx_st[b, k, 0:STATE, :].astype(F32)
+        for k in range(n_sp):
+            if k != owner:
+                to_owner(lat_st, b, k, lm_send, lm_recv).wait_recv()
+        for k in order:
+            entry = state.astype(BF16)
+            if k == owner:
+                ent_rx[b] = entry
+            else:
+                ent_tx[b, k] = entry
+                entry_copy(b, k).start()
+            state = growth(lat_st, b, k) * state + lat_st[b, k, 0:STATE, :].astype(F32)
+
+    for b, (d, g, owner) in enumerate(blocks):
+        pl.when(s == owner)(functools.partial(scan_block, b, d, owner))
+    for b, (d, g, owner) in enumerate(blocks):
+        pl.when(s != owner)(entry_copy(b, s).wait_recv)
+    mixed_y = y_loc[...]
+    zero_block = jnp.zeros((STATE, repeat_cols), BF16)
     for d in range(2):
-        acc = [jnp.zeros((1, repeat_cols), F32) for _ in range(groups)]
-        state = [jnp.zeros((STATE, repeat_cols), F32) for _ in range(groups)]
-        for k in range(n_sp):
-            place = n_sp - 1 - k if d == 0 else k
-            slot = lax.rem(s + n_sp - place, n_sp)
-            tot = totals(ctx_msg[slot, d, trows, :])
-            for g in range(groups):
-                state[g] = state[g] + jnp.exp(acc[g]) * ctx_msg[slot, d, srows[g], :].astype(F32)
-                acc[g] = acc[g] + tot[g]
-        start.append(state)
-    for c in lm:
-        c.wait_recv()
-    mixed_y = y_loc[...]
-    for d in range(2):
-        acc = [jnp.zeros((1, repeat_cols), F32) for _ in range(groups)]
-        state = [jnp.zeros((STATE, repeat_cols), F32) for _ in range(groups)]
-        for e in range(1, n_sp):
-            slot = e if d == 0 else n_sp - e
-            valid = (s >= e) if d == 0 else (s + e < n_sp)
-            live = jnp.where(valid, 1.0, 0.0)
-            tot = totals(lat_rx[slot, trows, :])
-            for g in range(groups):
-                state[g] = state[g] + live * (
-                    jnp.exp(acc[g]) * lat_rx[slot, srows[g], :].astype(F32)
+        entry_all = jnp.concatenate(
+            [
+                jnp.concatenate(
+                    [ent_rx[d * groups + g] if k == g else zero_block for k in range(groups)],
+                    axis=1,
                 )
-                acc[g] = acc[g] + live * tot[g]
-        blocks = []
-        for g in range(groups):
-            entry = (state[g] + jnp.exp(acc[g]) * start[d][g]).astype(BF16)
-            pieces = [
-                entry if k == g else jnp.zeros((STATE, repeat_cols), BF16) for k in range(groups)
-            ]
-            blocks.append(jnp.concatenate(pieces, axis=1) if groups > 1 else entry)
-        entry_all = jnp.concatenate(blocks, axis=0) if groups > 1 else blocks[0]
+                for g in range(groups)
+            ],
+            axis=0,
+        )
         mixed_y = mixed_y + reach[:, d * head_cols:(d + 1) * head_cols] * dot(lat_c, entry_all)
     gated = mixed_y * gate_act
     og_row = flat_row(og[...].astype(F32))
@@ -437,8 +437,21 @@
     final = pltpu.make_async_copy(out_v, out_h, out_sem)
     final.start()
 
-    for c in tok + ctx_halo + cm + lm + nm:
+    for c in tok + ctx_halo + nm:
         c.wait_send()
+
+    def sent(b, owner):
+        to_owner(ctx_st, b, s, cm_send, cm_recv).wait_send()
+        to_owner(lat_st, b, s, lm_send, lm_recv).wait_send()
+
+    def handed(b, owner):
+        for k in range(n_sp):
+            if k != owner:
+                entry_copy(b, k).wait_send()
+
+    for b, (d, g, owner) in enumerate(blocks):
+        pl.when(s != owner)(functools.partial(sent, b, owner))
+        pl.when(s == owner)(functools.partial(handed, b, owner))
 
     @pl.when(t == n_tp - 1)
     def _():
@@ -489,7 +502,7 @@
     V = pltpu.VMEM
     D = pltpu.SemaphoreType.DMA
     held = [args[i] for i in (0, 3, 4, 5, 6, 7, 8, 9, 10, 11, 12, 13, 14, 15, 16, 17)]
-    msg = (groups * STATE + 16, repeat_cols)
+    count = 2 * groups
     scratch = [V(a.shape, a.dtype) for a in held] + [
         V((2, width // LANES, LANES), F32),
         V((LANES, width), BF16),
@@ -504,9 +517,10 @@
         V((reducers, 2, chunk), F32),
         V((length + HALO, width), BF16),
         V((ctx_len + HALO, width), BF16),
-        V((n_sp, 2) + msg, BF16),
-        V((2,) + msg, BF16),
-        V((n_sp,) + msg, BF16),
+        V((count, n_sp, STATE + 16, repeat_cols), BF16),
+        V((count, n_sp, STATE + 16, repeat_cols), BF16),
+        V((count, n_sp, STATE, repeat_cols), BF16),
+        V((count, STATE, repeat_cols), BF16),
         V((length, head_cols), F32),
         V((length, head_cols), BF16),
         V((n_tp, rows, head_cols), BF16),
@@ -516,7 +530,8 @@
         D((4,)),
         D((n_tp,)), D((n_tp,)),
         D((n,)), D((n,)), D((n,)), D((n,)),
-        D((n_sp,)), D((n_sp,)), D((n_sp,)), D((n_sp,)),
+        D((count,)), D((count * n_sp,)), D((count,)), D((count * n_sp,)),
+        D((count * n_sp,)), D((count,)),
         D((n_tp,)), D((n_tp,)),
         D,
     ]

time: 47 us -> 42.4 us (0.902)
  Pallas kernels: 45.2 us -> 40.6 us
    pallas_call x1, Pallas kernels: 45.2 us -> 40.6 us  [local(): pl.pallas_call(functools.partial(mixer_kernel, n_sp, n_tp, reducers), out...]
where the time goes in v3:
time: 42.4 us; the launch traced here: 42.3 us
  Pallas kernels  40.6 us (96%)
  local copies, waits for them, and re-layouts  1.67 us (4%)
    pallas_call x1, Pallas kernels, local(): pl.pallas_call(functools.partial(mixer_kernel, n_sp, n_tp, reducers), out...  40.6 us
    unnamed x1, local copies, waits for them, and re-layouts  1.67 us

profile of v3, /device:TPU:0, one launch (start us, length us, event | category | flops | bytes accessed | tf_op | source)
XLA Modules:
  0.0 42.3 jit_solution(755852565715342103)
XLA Ops:
  0.0 40.6 %shard_map.172 = bf16[64,2048]{1,0:T(8,128)(2,1)} custom-call(bf16[16,128]{1,0:T(8,128)(2,1)} %bitcast.7, bf16[64,2048]{1,0:T(8,128)(2,1)} %latent_h.1, bf16[128,2048]{1,0:T(8,128)(2,1)} %context_h.1, bf16[256,6144]{1,0:T(8,128)(2,1)} %modulation_h.1, bf16[16,128]{1,0:T(8,128)(2,1)} %bitcast.8, bf16[2048,512]{1,0:T(8,128)(2,1)} %wx_h.1, ...), custom_call_target="tpu_custom_call" | custom-call | tf_op jit(solution)/shard_map/pallas_call | solution.py:538
  40.6 1.7 %copy.20 = bf16[64,2048]{1,0:T(8,128)(2,1)} copy(bf16[64,2048]{1,0:T(8,128)(2,1)} %shard_map.172) | data formatting | bytes 524288

commit v4 on v3

--- a/solution.py
+++ b/solution.py
@@ -131,6 +131,25 @@
 
     after = lax.rem(s + 1, n_sp)
     before = lax.rem(s + n_sp - 1, n_sp)
+    loads[0].wait()
+    loads[16].wait()
+    cond_rows[0] = silu(cond[...].astype(F32))
+    cond_rows[1] = silu(ccond[...].astype(F32))
+    own = [own_cond(cond_rows, k, rank, mod_w.shape[0]) for k in range(2)]
+    pick = iota((16, mod_w.shape[0]), 0)
+    cols = jnp.where(pick == 0, own[0], jnp.where(pick == 1, own[1], 0.0)).astype(BF16)
+    loads[1].wait()
+    full = reducers == n
+    partial = dot(cols, mod_w[...])
+    for i in range(reducers):
+        part[i] = partial[0:2, i * chunk:(i + 1) * chunk]
+    rs = []
+    for d in range(1, n):
+        other = lax.rem(rank + d, n)
+        rs.append(remote(part.at[lax.rem(other, reducers)], part_rx.at[d], rs_send.at[d],
+                         rs_recv.at[d], group_peer(d)))
+        guarded(full, other < reducers, rs[-1].start)
+
     tok = []
     for d in range(1, n_tp):
         c = remote(latent_h, lat.at[own_rows], tok_send.at[d], tok_recv.at[d],
@@ -159,25 +178,6 @@
     def _():
         for c in high:
             c.start()
-
-    loads[0].wait()
-    loads[16].wait()
-    cond_rows[0] = silu(cond[...].astype(F32))
-    cond_rows[1] = silu(ccond[...].astype(F32))
-    own = [own_cond(cond_rows, k, rank, mod_w.shape[0]) for k in range(2)]
-    pick = iota((16, mod_w.shape[0]), 0)
-    cols = jnp.where(pick == 0, own[0], jnp.where(pick == 1, own[1], 0.0)).astype(BF16)
-    loads[1].wait()
-    full = reducers == n
-    partial = dot(cols, mod_w[...])
-    for i in range(reducers):
-        part[i] = partial[0:2, i * chunk:(i + 1) * chunk]
-    rs = []
-    for d in range(1, n):
-        other = lax.rem(rank + d, n)
-        rs.append(remote(part.at[lax.rem(other, reducers)], part_rx.at[d], rs_send.at[d],
-                         rs_recv.at[d], group_peer(d)))
-        guarded(full, other < reducers, rs[-1].start)
 
     for i in (2, 3, 4):
         loads[i].wait()

time: 42.4 us -> 41.2 us (0.972)
  Pallas kernels: 40.6 us -> 39.4 us
    pallas_call x1, Pallas kernels: 40.6 us -> 39.4 us  [local(): pl.pallas_call(functools.partial(mixer_kernel, n_sp, n_tp, reducers), out...]
where the time goes in v4:
time: 41.2 us; the launch traced here: 41.1 us
  Pallas kernels  39.4 us (96%)
  local copies, waits for them, and re-layouts  1.67 us (4%)
    pallas_call x1, Pallas kernels, local(): pl.pallas_call(functools.partial(mixer_kernel, n_sp, n_tp, reducers), out...  39.4 us
    unnamed x1, local copies, waits for them, and re-layouts  1.67 us

profile of v4, /device:TPU:0, one launch (start us, length us, event | category | flops | bytes accessed | tf_op | source)
XLA Modules:
  0.0 41.1 jit_solution(5599658562695473023)
XLA Ops:
  0.0 39.4 %shard_map.172 = bf16[64,2048]{1,0:T(8,128)(2,1)} custom-call(bf16[16,128]{1,0:T(8,128)(2,1)} %bitcast.7, bf16[64,2048]{1,0:T(8,128)(2,1)} %latent_h.1, bf16[128,2048]{1,0:T(8,128)(2,1)} %context_h.1, bf16[256,6144]{1,0:T(8,128)(2,1)} %modulation_h.1, bf16[16,128]{1,0:T(8,128)(2,1)} %bitcast.8, bf16[2048,512]{1,0:T(8,128)(2,1)} %wx_h.1, ...), custom_call_target="tpu_custom_call" | custom-call | tf_op jit(solution)/shard_map/pallas_call | solution.py:538
  39.4 1.7 %copy.20 = bf16[64,2048]{1,0:T(8,128)(2,1)} copy(bf16[64,2048]{1,0:T(8,128)(2,1)} %shard_map.172) | data formatting | bytes 524288
